TPU v7x, 32 devices: a whole 2x2x4 slice. The times are simulated.
32 devices in a mesh: ep: 16 (over z, y, core), tp: 2 (over x).
Axes of the slice: x: 2, y: 2, z: 4, core: 2. Of those that a mesh axis runs over, the one named last changes fastest.
Arguments:
- tokens: bfloat16 [2048, 2048], P('ep'), may hold values from -6 to 6
- expert_ids: int32 [2048, 2], P('ep'), may hold values from 0 to 15, as said below
- route_weights: bfloat16 [2048, 2], P('ep'), may hold values from 0.099609375 to 1
- cotangent: bfloat16 [2048, 2048], P('ep'), may hold values from -3 to 3
- w_gate: bfloat16 [16, 2048, 512], P('ep', None, 'tp'), may hold values from -0.125 to 0.125
- w_up: bfloat16 [16, 2048, 512], P('ep', None, 'tp'), may hold values from -0.125 to 0.125
- w_down: bfloat16 [16, 512, 2048], P('ep', 'tp'), may hold values from -0.25 to 0.25
Outputs:
- token_grad: bfloat16 [2048, 2048], P('ep', 'tp')
- route_grad: bfloat16 [2048, 2], P('ep')
- grad_gate: bfloat16 [16, 2048, 512], P('ep', None, 'tp')
- grad_up: bfloat16 [16, 2048, 512], P('ep', None, 'tp')
- grad_down: bfloat16 [16, 512, 2048], P('ep', 'tp')
- gate_rows: float32 [16, 2048], P('ep')
- up_rows: float32 [16, 2048], P('ep')
- down_rows: float32 [16, 512], P('ep', 'tp')
Inputs may be any that keep to these rules, and one draw needn't show every extreme that they name: `expert_ids`: each row names 2 different experts of one group: both lie in g * 4 to (g + 1) * 4 - 1 for the row's group g. In the rows of one device (aligned blocks of 128 rows) no expert is named more than 32 times, and in every block some expert is named exactly 32 times.
All inputs are finite; a program needn't handle non-finite values.
Results may differ from a plain program's by a relative error of at most 0.012.
Values may be sent and summed in bfloat16 or wider, within the bound.
A program may use at most 64 MiB of HBM per device.

v0:
```python
import jax
import jax.numpy as jnp
from jax import lax
from jax.sharding import PartitionSpec as P

TOPK = 2


def on_device(tokens, expert_ids, route_weights, cotangent, w_gate, w_up, w_down):
    tok_rows, model_width = tokens.shape
    experts = lax.axis_size("ep")
    splits = lax.axis_size("tp")
    capacity = 2 * tok_rows * TOPK // experts
    slot_count = experts * capacity
    assigns = tok_rows * TOPK
    flat_ids = expert_ids.reshape(-1)
    onehot = (flat_ids[:, None] == jnp.arange(experts, dtype=jnp.int32)[None, :]).astype(
        jnp.float32
    )
    assign_order = jnp.arange(assigns, dtype=jnp.int32)
    earlier = (assign_order[:, None] > assign_order[None, :]).astype(jnp.float32)
    before = jnp.dot(earlier, onehot, precision=lax.Precision.HIGHEST)
    slot_rank = jnp.sum(before * onehot, axis=1).astype(jnp.int32)
    position = flat_ids * capacity + slot_rank
    slot_owner = jnp.full((slot_count,), tok_rows, jnp.int32).at[position].set(assign_order // TOPK)
    slot_scale = jnp.zeros((slot_count,), jnp.bfloat16).at[position].set(route_weights.reshape(-1))
    slice_width = model_width // splits
    slice_start = lax.axis_index("tp") * slice_width
    rows_slice = lax.dynamic_slice_in_dim(tokens, slice_start, slice_width, 1)
    cot_slice = lax.dynamic_slice_in_dim(cotangent, slice_start, slice_width, 1)
    rows_pad = jnp.concatenate([rows_slice, jnp.zeros((1, slice_width), jnp.bfloat16)], axis=0)
    cot_pad = jnp.concatenate([cot_slice, jnp.zeros((1, slice_width), jnp.bfloat16)], axis=0)
    outgoing = rows_pad[slot_owner]
    outgoing_cot = cot_pad[slot_owner]
    part_rows, part_cot, got_scale = (
        lax.all_to_all(outgoing, "ep", split_axis=0, concat_axis=0, tiled=True),
        lax.all_to_all(outgoing_cot, "ep", split_axis=0, concat_axis=0, tiled=True),
        lax.all_to_all(slot_scale, "ep", split_axis=0, concat_axis=0, tiled=True),
    )
    slot_rows, slot_cot = (
        lax.all_gather(part_rows, "tp", axis=1, tiled=True),
        lax.all_gather(part_cot, "tp", axis=1, tiled=True),
    )
    scale_col = got_scale.reshape(slot_count, 1).astype(jnp.float32)
    gate_cols = w_gate[0]
    up_cols = w_up[0]
    down_part = w_down[0]
    gate_pre = jnp.dot(slot_rows, gate_cols, preferred_element_type=jnp.float32)
    up_pre = jnp.dot(slot_rows, up_cols, preferred_element_type=jnp.float32)
    hidden_back = lax.dot_general(
        slot_cot, down_part, (((1,), (1,)), ((), ())), preferred_element_type=jnp.float32
    )
    gate_sig = jax.nn.sigmoid(gate_pre)
    activated = gate_pre * gate_sig
    hidden = activated * up_pre
    route_part = jnp.sum(hidden * hidden_back, axis=1)
    hidden_cot = scale_col * hidden_back
    up_cot = (hidden_cot * activated).astype(jnp.bfloat16)
    gate_cot = (hidden_cot * up_pre * gate_sig * (1.0 + gate_pre * (1.0 - gate_sig))).astype(
        jnp.bfloat16
    )
    weighted_hidden = (scale_col * hidden).astype(jnp.bfloat16)
    grad_down = lax.dot_general(
        weighted_hidden, slot_cot, (((0,), (0,)), ((), ())), preferred_element_type=jnp.float32
    ).astype(jnp.bfloat16)
    grad_gate = lax.dot_general(
        slot_rows, gate_cot, (((0,), (0,)), ((), ())), preferred_element_type=jnp.float32
    ).astype(jnp.bfloat16)
    grad_up = lax.dot_general(
        slot_rows, up_cot, (((0,), (0,)), ((), ())), preferred_element_type=jnp.float32
    ).astype(jnp.bfloat16)
    token_term = lax.dot_general(
        gate_cot, gate_cols, (((1,), (1,)), ((), ())), preferred_element_type=jnp.float32
    )
    token_term = token_term + lax.dot_general(
        up_cot, up_cols, (((1,), (1,)), ((), ())), preferred_element_type=jnp.float32
    )
    reduced = lax.psum_scatter(
        token_term.astype(jnp.bfloat16), "tp", scatter_dimension=1, tiled=True
    )
    gate_square = jnp.sum(jnp.square(grad_gate.astype(jnp.float32)), axis=1)
    up_square = jnp.sum(jnp.square(grad_up.astype(jnp.float32)), axis=1)
    down_square = jnp.sum(jnp.square(grad_down.astype(jnp.float32)), axis=1)
    route_total, gate_rows, up_rows = lax.psum((route_part, gate_square, up_square), "tp")
    back_rows, back_route = (
        lax.all_to_all(reduced, "ep", split_axis=0, concat_axis=0, tiled=True),
        lax.all_to_all(
            route_total.astype(jnp.bfloat16), "ep", split_axis=0, concat_axis=0, tiled=True
        ),
    )
    per_assign = back_rows[position].astype(jnp.float32).reshape(tok_rows, TOPK, -1)
    token_grad = jnp.sum(per_assign, axis=1).astype(jnp.bfloat16)
    route_grad = back_route[position].reshape(tok_rows, TOPK)
    return (
        token_grad,
        route_grad,
        grad_gate[None],
        grad_up[None],
        grad_down[None],
        gate_rows[None],
        up_rows[None],
        down_square[None],
    )


def solution(mesh):
    return jax.shard_map(
        on_device,
        mesh=mesh,
        in_specs=(
            P("ep", None),
            P("ep", None),
            P("ep", None),
            P("ep", None),
            P("ep", None, "tp"),
            P("ep", None, "tp"),
            P("ep", "tp", None),
        ),
        out_specs=(
            P("ep", "tp"),
            P("ep", None),
            P("ep", None, "tp"),
            P("ep", None, "tp"),
            P("ep", "tp", None),
            P("ep", None),
            P("ep", None),
            P("ep", "tp"),
        ),
        check_vma=False,
    )
```

profile of v0, /device:TPU:9, one launch (start us, length us, event | category | flops | bytes accessed | tf_op | source)
XLA Modules:
  0.0 192.4 jit_solution(12211207150902373876)
XLA Ops:
  9.4 1.4 scatter_custom_fusion.1
  11.9 2.1 %gather_fusion.1 = bf16[512,1024]{1,0:T(8,128)(2,1)S(1)} fusion(bf16[129,1024]{1,0:T(8,128)(2,1)S(1)} %concatenate.7, s32[1024]{0:T(1024)S(1)} %pad_clamp_fusion.1), kind=kCustom, calls=%fused_computation.1 | custom fusion | bytes 2099200 | tf_op jit(solution)/shard_map/gather | solution.py:33
  14.0 31.8 %all_to_all.59 = bf16[16,32,1024]{2,1,0:T(8,128)(2,1)} all-to-all(bf16[16,32,1024]{2,1,0:T(8,128)(2,1)S(1)} %bitcast.43), channel_id=1, replica_groups=mesh['ep'=16,'tp'=2] {'ep'}, dimensions={0} | all-to-all | bytes 2097152 | tf_op jit(solution)/shard_map/all_to_all | solution.py:36
  45.9 2.1 %gather_fusion = bf16[512,1024]{1,0:T(8,128)(2,1)S(1)} fusion(bf16[129,1024]{1,0:T(8,128)(2,1)S(1)} %concatenate.6, s32[1024]{0:T(1024)S(1)} %pad_clamp_fusion.1), kind=kCustom, calls=%fused_computation | custom fusion | bytes 2099200 | tf_op jit(solution)/shard_map/gather | solution.py:34
  48.0 29.6 %all_to_all.60 = bf16[16,32,1024]{2,1,0:T(8,128)(2,1)} all-to-all(bf16[16,32,1024]{2,1,0:T(8,128)(2,1)S(1)} %bitcast.42), channel_id=1, replica_groups=mesh['ep'=16,'tp'=2] {'ep'}, dimensions={0} | all-to-all | bytes 2097152 | tf_op jit(solution)/shard_map/all_to_all | solution.py:37
  78.0 2.2 %scatter_custom_fusion = bf16[512]{0:T(512)(128)(2,1)S(1)} fusion(s32[256]{0:T(256)S(1)} %bitcast.52, bf16[256]{0:T(256)(128)(2,1)S(1)} %reshape.116, bf16[]{:T(256)} %constant.13.clone.1), kind=kCustom, calls=%fused_computation.49 | custom fusion | bytes 1026 | tf_op jit(solution)/shard_map/scatter | solution.py:26
  80.3 8.9 %all_to_all.61 = bf16[16,32,1]{1,2,0:T(2,128)(2,1)S(1)} all-to-all(bf16[16,32,1]{1,2,0:T(2,128)(2,1)S(1)} %all_to_all.52), channel_id=1, replica_groups=mesh['ep'=16,'tp'=2] {'ep'}, dimensions={0} | all-to-all | bytes 2048 | tf_op jit(solution)/shard_map/all_to_all | solution.py:38
  89.3 2.6 %fusion.3 = f32[512,256]{0,1:T(8,128)S(1)} fusion(bf16[512,2048]{1,0:T(8,128)(2,1)} %all-gather.5.cloned.1.call-done, bf16[1,2048,256]{2,1,0:T(8,128)(2,1)S(1)} %copy-done), kind=kOutput, calls=%fused_computation.17 | convolution fusion | flops 536870912 | bytes 3670016 | tf_op jit(solution)/shard_map/dot_general | solution.py:48
  91.9 1.6 fusion.6
  93.5 19.1 %all-gather.3.cloned.1.call-done = bf16[512,2048]{1,0:T(8,128)(2,1)} async-done(((bf16[512,1024]{1,0:T(8,128)(2,1)}), bf16[512,2048]{1,0:T(8,128)(2,1)}) %all-gather.3.cloned.1.call-update) | async-done | bytes 2097168 | tf_op jit(solution)/shard_map/all_gather | solution.py:42
  112.6 2.9 %multiply_reduce_fusion.3 = (f32[512]{0:T(512)S(1)}, bf16[512,256]{0,1:T(8,128)(2,1)S(1)}, bf16[512,256]{0,1:T(8,128)(2,1)S(1)}) fusion(f32[512,256]{0,1:T(8,128)} %fusion.6, f32[512,256]{0,1:T(8,128)S(1)} %fusion.3, f32[512]{0:T(512)S(1)} %reshape.79, bf16[512,2048]{1,0:T(8,128)(2,1)} %all-gather.3.cloned.1.call-done, bf16[1,256,2048]{2,1,0:T(8,128)(2,1)} %param.13), kind=kOutput, calls=%fused_computation.25 | convolution fusion | flops 539098624 | bytes 4722688 | tf_op jit(solution)/shard_map/dot_general | solution.py:50
  116.3 2.1 %add_convert_fusion = bf16[512,2048]{1,0:T(8,128)(2,1)} fusion(f32[512,2048]{1,0:T(8,128)S(1)} %fusion.1, bf16[512,256]{0,1:T(8,128)(2,1)S(1)} %get-tuple-element.37, bf16[1,2048,256]{2,1,0:T(8,128)(2,1)S(1)} %copy-done.1), kind=kOutput, calls=%fused_computation.6 | convolution fusion | flops 538968064 | bytes 7602176 | tf_op jit(solution)/shard_map/dot_general | solution.py:75
  118.5 2.5 %multiply_reduce_fusion.2 = (f32[2048]{0:T(1024)S(1)}, bf16[2048,256]{0,1:T(8,128)(2,1)S(1)}) fusion(bf16[512,256]{0,1:T(8,128)(2,1)S(1)} %get-tuple-element.36, bf16[512,2048]{1,0:T(8,128)(2,1)} %all-gather.5.cloned.1.call-done), kind=kOutput, calls=%fused_computation.12 | convolution fusion | flops 538966016 | bytes 3416064 | tf_op jit(solution)/shard_map/dot_general | solution.py:66
  121.0 1.7 multiply_reduce_fusion.1
  122.7 6.5 %all-reduce.2 = (bf16[512]{0:T(512)(128)(2,1)S(1)}, f32[1,2048]{1,0:T(1,128)}, f32[1,2048]{1,0:T(1,128)}) all-reduce(f32[512]{0:T(512)S(1)} %get-tuple-element.35, f32[1,2048]{1,0:T(1,128)S(1)} %bitcast.49, f32[1,2048]{1,0:T(1,128)S(1)} %bitcast.50), channel_id=1, replica_groups=mesh['ep'=16,'tp'=2] {'tp'}, use_global_device_ids=true, to_apply=%region_6.7 | all-reduce | flops 4608 | bytes 35840 | tf_op jit(solution)/shard_map/psum | solution.py:84
  129.3 13.0 %all_to_all.62 = bf16[16,32,1]{1,2,0:T(2,128)(2,1)S(1)} all-to-all(bf16[16,32,1]{1,2,0:T(2,128)(2,1)S(1)} %all_to_all.53), channel_id=1, replica_groups=mesh['ep'=16,'tp'=2] {'ep'}, dimensions={0} | all-to-all | bytes 2048 | tf_op jit(solution)/shard_map/all_to_all | solution.py:87
  142.3 8.7 %reduce-scatter.2.cloned.1.call-done = bf16[512,1024]{1,0:T(8,128)(2,1)} async-done(((bf16[512,2048]{1,0:T(8,128)(2,1)}), bf16[512,1024]{1,0:T(8,128)(2,1)}) %reduce-scatter.2.cloned.1.call-update) | async-done | bytes 1048592 | tf_op jit(solution)/shard_map/reduce_scatter | solution.py:78
  150.9 6.5 %all-to-all-start.3 = ((bf16[16,32,1024]{2,1,0:T(8,128)(2,1)}), bf16[16,32,1024]{2,1,0:T(8,128)(2,1)S(1)}, u32[]{:S(2)}, u32[]{:S(2)}) async-start(bf16[16,32,1024]{2,1,0:T(8,128)(2,1)} %bitcast.46), calls=%async_computation.4 | async-start | bytes 2097152 | tf_op jit(solution)/shard_map/all_to_all | solution.py:86
  157.5 2.3 %copy.30 = bf16[1,2048,256]{2,1,0:T(8,128)(2,1)} copy(bf16[1,2048,256]{1,2,0:T(8,128)(2,1)} %bitcast.48) | data formatting | bytes 2097152
  159.7 1.3 copy.29
  161.0 4.2 %multiply_reduce_fusion = (f32[256]{0:T(256)}, bf16[256,2048]{1,0:T(8,128)(2,1)}) fusion(bf16[512,2048]{1,0:T(8,128)(2,1)} %all-gather.3.cloned.1.call-done, f32[512]{0:T(512)S(1)} %reshape.79, f32[512,256]{0,1:T(8,128)} %fusion.6, f32[512,256]{0,1:T(8,128)} %copy-done.5), kind=kOutput, calls=%fused_computation.10 | convolution fusion | flops 539885312 | bytes 4197376 | tf_op jit(solution)/shard_map/dot_general | solution.py:63
  165.4 1.9 %gather_fusion.3 = bf16[256]{0:T(256)(128)(2,1)S(1)} fusion(bf16[512]{0:T(512)(128)(2,1)S(1)} %all_to_all.51, s32[1024]{0:T(1024)S(1)} %pad_clamp_fusion), kind=kCustom, calls=%fused_computation.3 | custom fusion | bytes 2048 | tf_op jit(solution)/shard_map/gather | solution.py:93
  168.1 14.3 %all-to-all-done.3 = bf16[16,32,1024]{2,1,0:T(8,128)(2,1)S(1)} async-done(((bf16[16,32,1024]{2,1,0:T(8,128)(2,1)}), bf16[16,32,1024]{2,1,0:T(8,128)(2,1)S(1)}, u32[]{:S(2)}, u32[]{:S(2)}) %all-to-all-start.3) | async-done | bytes 1048608 | tf_op jit(solution)/shard_map/all_to_all | solution.py:86
  183.7 2.1 %reduce_sum.58 = bf16[128,1024]{1,0:T(8,128)(2,1)} reduce(bf16[128,2,1024]{2,1,0:T(2,128)(2,1)S(1)} %gather.17, bf16[]{:T(256)} %constant.13.clone.1), dimensions={1}, to_apply=%region_4.5 | reduce | flops 131072 | bytes 786434 | tf_op jit(solution)/shard_map/reduce_sum | solution.py:92
  (47 shorter events, 7.1 us)
Async XLA Ops:
  7.2 82.1 %copy-start = (bf16[1,2048,256]{2,1,0:T(8,128)(2,1)S(1)}, bf16[1,2048,256]{2,1,0:T(8,128)(2,1)}, u32[]{:S(2)}) copy-start(bf16[1,2048,256]{2,1,0:T(8,128)(2,1)} %param.11) | copy-start | bytes 3145732
  7.2 82.1 %all-gather.5.cloned.1.call-start = ((), (), s32[]{:S(2)}) async-start(), calls=%async_computation.7 | async-start | bytes 3145728 | tf_op jit(solution)/shard_map/all_gather | solution.py:41
  45.9 66.7 %all-gather.3.cloned.1.call-start = ((), (), s32[]{:S(2)}) async-start(), calls=%async_computation.6 | async-start | bytes 3145728 | tf_op jit(solution)/shard_map/all_gather | solution.py:42
  48.0 29.7 %copy-start.2 = (bf16[128,2]{0,1:T(2,128)(2,1)S(1)}, bf16[128,2]{0,1:T(2,128)(2,1)}, u32[]{:S(2)}) copy-start(bf16[128,2]{0,1:T(2,128)(2,1)} %param.9) | copy-start | bytes 1540
  77.7 14.2 %copy-start.1 = (bf16[1,2048,256]{2,1,0:T(8,128)(2,1)S(1)}, bf16[1,2048,256]{2,1,0:T(8,128)(2,1)}, u32[]{:S(2)}) copy-start(bf16[1,2048,256]{2,1,0:T(8,128)(2,1)} %param.12) | copy-start | bytes 3145732
  77.7 73.3 %reduce-scatter.2.cloned.1.call-start = ((), (), s32[]{:S(2)}) async-start(), calls=%async_computation.8 | async-start | bytes 3145728 | tf_op jit(solution)/shard_map/reduce_scatter | solution.py:78
  89.3 2.6 %copy-start.3 = (bf16[512,2048]{1,0:T(8,128)(2,1)S(1)}, bf16[512,2048]{1,0:T(8,128)(2,1)}, u32[]{:S(2)}) copy-start(bf16[512,2048]{1,0:T(8,128)(2,1)} %all-gather.5.cloned.1.call-done) | copy-start | bytes 6291460
  91.9 23.6 %copy-start.5 = (f32[512,256]{0,1:T(8,128)}, f32[512,256]{0,1:T(8,128)S(1)}, u32[]{:S(2)}) copy-start(f32[512,256]{0,1:T(8,128)S(1)} %fusion.3) | copy-start | bytes 1572868
  118.5 2.5 %copy-start.4 = (bf16[512,2048]{1,0:T(8,128)(2,1)S(1)}, bf16[512,2048]{1,0:T(8,128)(2,1)}, u32[]{:S(2)}) copy-start(bf16[512,2048]{1,0:T(8,128)(2,1)} %all-gather.5.cloned.1.call-done) | copy-start | bytes 6291460
  150.9 31.4 %all-to-all-start.3 = ((bf16[16,32,1024]{2,1,0:T(8,128)(2,1)}), bf16[16,32,1024]{2,1,0:T(8,128)(2,1)S(1)}, u32[]{:S(2)}, u32[]{:S(2)}) async-start(bf16[16,32,1024]{2,1,0:T(8,128)(2,1)} %bitcast.46), calls=%async_computation.4 | async-start | bytes 2097152 | tf_op jit(solution)/shard_map/all_to_all | solution.py:86
Sparse Core Ops, SparseCore 0:
  46.0 31.9 all-gather.4
  79.5 33.0 all-gather.2
  118.6 32.2 reduce-scatter.1
where the time goes:
time: 193 us; the launch traced here: 192 us
  blocking collectives  89.8 us (47%)
  waiting for transfers between devices  42.1 us (22%)
  matrix products  18.6 us (10%)
  local copies, waits for them, and re-layouts  18.2 us (9%)
  between operations  14 us (7%)
  starting transfers between devices  6.63 us (3%)
  other arithmetic  3 us (2%)
    all_to_all x1, blocking collectives, on_device(): lax.all_to_all(outgoing, 'ep', split_axis=0, concat_axis=0, tiled=True)  31.8 us
    all_to_all x1, blocking collectives, on_device(): lax.all_to_all(outgoing_cot, 'ep', split_axis=0, concat_axis=0, tiled=True)  29.6 us
    all_gather x1, waiting for transfers between devices, on_device(): lax.all_gather(part_cot, 'tp', axis=1, tiled=True)  19.1 us
    all_to_all x1, waiting for transfers between devices, on_device(): lax.all_to_all(reduced, 'ep', split_axis=0, concat_axis=0, tiled=True)  14.3 us
    all_to_all x1, blocking collectives, on_device(): lax.all_to_all(route_total.astype(jnp.bfloat16), 'ep', split_axis=0, conc...  13 us
    all_to_all x1, blocking collectives, on_device(): lax.all_to_all(slot_scale, 'ep', split_axis=0, concat_axis=0, tiled=True)  8.9 us
    reduce_scatter x1, waiting for transfers between devices, on_device(): lax.psum_scatter(token_term.astype(jnp.bfloat16), 'tp', scatter_dimension...  8.67 us
    psum x1, blocking collectives, on_device(): lax.psum((route_part, gate_square, up_square), 'tp')  6.52 us
  transfers between devices with their start and end apart: 4, of which 3 were waited for; matrix products, arithmetic and copies ran while one was open for 12% of the time, Pallas kernels for 0%

commit v1 on v0

--- a/solution.py
+++ b/solution.py
@@ -39,7 +39,7 @@
     )
     slot_rows, slot_cot = (
         lax.all_gather(part_rows, "tp", axis=1, tiled=True),
-        lax.all_gather(part_cot, "tp", axis=1, tiled=True),
+        jnp.concatenate(lax.all_gather(part_cot, "tp"), axis=1),
     )
     scale_col = got_scale.reshape(slot_count, 1).astype(jnp.float32)
     gate_cols = w_gate[0]

time: 193 us -> 195 us (1.010)
  local copies, waits for them, and re-layouts: 18.2 us -> 21.8 us
  matrix products: 18.6 us -> 15.6 us
    all_gather x1, waiting for transfers between devices: 0.01 us -> 20.4 us  [on_device(): lax.all_gather(part_rows, 'tp', axis=1, tiled=True)]
    all_gather x1, waiting for transfers between devices: 19.1 us -> 0.01 us  [on_device(): lax.all_gather(part_cot, 'tp')]
    all_gather x0 -> x1, local copies, waits for them, and re-layouts: none -> 2.93 us  [on_device(): lax.all_gather(part_cot, 'tp')]
    all_to_all x1, blocking collectives: 29.6 us -> 31.8 us  [on_device(): lax.all_to_all(outgoing_cot, 'ep', split_axis=0, concat_axis=0, tiled=True)]
    all_to_all x1, blocking collectives: 31.8 us -> 29.6 us  [on_device(): lax.all_to_all(outgoing, 'ep', split_axis=0, concat_axis=0, tiled=True)]
    dot_general x1, matrix products: 2.94 us -> 0.92 us  [on_device(): lax.dot_general(slot_cot, down_part, (((1,), (1,)), ((), ())), preferred_...]
    unnamed x17 -> x27, local copies, waits for them, and re-layouts: 5.12 us -> 5.8 us
  transfers between devices with their start and end apart: 4 -> 4, of which waited for: 3 -> 3; matrix products, arithmetic and copies ran while one was open for 12% -> 11% of each run, Pallas kernels for 0% -> 0%
where the time goes in v1:
time: 195 us; the launch traced here: 194 us
  blocking collectives  89.8 us (46%)
  waiting for transfers between devices  43.4 us (22%)
  local copies, waits for them, and re-layouts  21.8 us (11%)
  matrix products  15.6 us (8%)
  between operations  14 us (7%)
  starting transfers between devices  6.63 us (3%)
  other arithmetic  2.94 us (2%)
    all_to_all x1, blocking collectives, on_device(): lax.all_to_all(outgoing_cot, 'ep', split_axis=0, concat_axis=0, tiled=True)  31.8 us
    all_to_all x1, blocking collectives, on_device(): lax.all_to_all(outgoing, 'ep', split_axis=0, concat_axis=0, tiled=True)  29.6 us
    all_gather x1, waiting for transfers between devices, on_device(): lax.all_gather(part_rows, 'tp', axis=1, tiled=True)  20.4 us
    all_to_all x1, waiting for transfers between devices, on_device(): lax.all_to_all(reduced, 'ep', split_axis=0, concat_axis=0, tiled=True)  14.3 us
    all_to_all x1, blocking collectives, on_device(): lax.all_to_all(route_total.astype(jnp.bfloat16), 'ep', split_axis=0, conc...  13 us
    all_to_all x1, blocking collectives, on_device(): lax.all_to_all(slot_scale, 'ep', split_axis=0, concat_axis=0, tiled=True)  8.9 us
    reduce_scatter x1, waiting for transfers between devices, on_device(): lax.psum_scatter(token_term.astype(jnp.bfloat16), 'tp', scatter_dimension...  8.68 us
    psum x1, blocking collectives, on_device(): lax.psum((route_part, gate_square, up_square), 'tp')  6.52 us
  transfers between devices with their start and end apart: 4, of which 3 were waited for; matrix products, arithmetic and copies ran while one was open for 11% of the time, Pallas kernels for 0%

profile of v1, /device:TPU:9, one launch (start us, length us, event | category | flops | bytes accessed | tf_op | source)
XLA Modules:
  0.0 194.3 jit_solution(3963568631655132502)
XLA Ops:
  9.4 1.4 scatter_custom_fusion.1
  11.9 2.1 %gather_fusion = bf16[512,1024]{1,0:T(8,128)(2,1)S(1)} fusion(bf16[129,1024]{1,0:T(8,128)(2,1)S(1)} %concatenate.6, s32[1024]{0:T(1024)S(1)} %pad_clamp_fusion.1), kind=kCustom, calls=%fused_computation | custom fusion | bytes 2099200 | tf_op jit(solution)/shard_map/gather | solution.py:34
  14.0 31.8 %all_to_all.56 = bf16[16,32,1024]{2,1,0:T(8,128)(2,1)} all-to-all(bf16[16,32,1024]{2,1,0:T(8,128)(2,1)S(1)} %bitcast.46), channel_id=1, replica_groups=mesh['ep'=16,'tp'=2] {'ep'}, dimensions={0} | all-to-all | bytes 2097152 | tf_op jit(solution)/shard_map/all_to_all | solution.py:37
  45.9 2.1 %gather_fusion.1 = bf16[512,1024]{1,0:T(8,128)(2,1)S(1)} fusion(bf16[129,1024]{1,0:T(8,128)(2,1)S(1)} %concatenate.7, s32[1024]{0:T(1024)S(1)} %pad_clamp_fusion.1), kind=kCustom, calls=%fused_computation.1 | custom fusion | bytes 2099200 | tf_op jit(solution)/shard_map/gather | solution.py:33
  48.0 29.6 %all_to_all.57 = bf16[16,32,1024]{2,1,0:T(8,128)(2,1)} all-to-all(bf16[16,32,1024]{2,1,0:T(8,128)(2,1)S(1)} %bitcast.45), channel_id=1, replica_groups=mesh['ep'=16,'tp'=2] {'ep'}, dimensions={0} | all-to-all | bytes 2097152 | tf_op jit(solution)/shard_map/all_to_all | solution.py:36
  78.0 2.2 %scatter_custom_fusion = bf16[512]{0:T(512)(128)(2,1)S(1)} fusion(s32[256]{0:T(256)S(1)} %bitcast.57, bf16[256]{0:T(256)(128)(2,1)S(1)} %reshape.125, bf16[]{:T(256)} %constant.13.clone.1), kind=kCustom, calls=%fused_computation.49 | custom fusion | bytes 1026 | tf_op jit(solution)/shard_map/scatter | solution.py:26
  80.3 8.9 %all_to_all.58 = bf16[16,32,1]{1,2,0:T(2,128)(2,1)S(1)} all-to-all(bf16[16,32,1]{1,2,0:T(2,128)(2,1)S(1)} %all_to_all.49), channel_id=1, replica_groups=mesh['ep'=16,'tp'=2] {'ep'}, dimensions={0} | all-to-all | bytes 2048 | tf_op jit(solution)/shard_map/all_to_all | solution.py:38
  89.3 2.9 %copy.35 = bf16[2,512,1024]{1,2,0:T(8,128)(2,1)S(1)} copy(bf16[2,512,1024]{2,1,0:T(8,128)(2,1)} %all-gather.3.cloned.1.call-done) | data formatting | bytes 4194304 | tf_op jit(solution)/shard_map/all_gather | solution.py:42
  92.2 20.4 %all-gather.5.cloned.1.call-done = bf16[512,2048]{1,0:T(8,128)(2,1)} async-done(((bf16[512,1024]{1,0:T(8,128)(2,1)}), bf16[512,2048]{1,0:T(8,128)(2,1)}) %all-gather.5.cloned.1.call-update) | async-done | bytes 2097168 | tf_op jit(solution)/shard_map/all_gather | solution.py:41
  112.6 2.5 %fusion.3 = f32[512,256]{0,1:T(8,128)S(1)} fusion(bf16[512,2048]{1,0:T(8,128)(2,1)} %all-gather.5.cloned.1.call-done, bf16[1,2048,256]{2,1,0:T(8,128)(2,1)S(1)} %copy-done), kind=kOutput, calls=%fused_computation.17 | convolution fusion | flops 536870912 | bytes 3670016 | tf_op jit(solution)/shard_map/dot_general | solution.py:48
  118.3 2.1 %add_convert_fusion = bf16[512,2048]{1,0:T(8,128)(2,1)} fusion(f32[512,2048]{1,0:T(8,128)S(1)} %fusion.1, bf16[512,256]{0,1:T(8,128)(2,1)S(1)} %get-tuple-element.45, bf16[1,2048,256]{2,1,0:T(8,128)(2,1)S(1)} %copy-done.2), kind=kOutput, calls=%fused_computation.6 | convolution fusion | flops 538968064 | bytes 7602176 | tf_op jit(solution)/shard_map/dot_general | solution.py:75
  120.4 2.5 %multiply_reduce_fusion.2 = (f32[2048]{0:T(1024)S(1)}, bf16[2048,256]{0,1:T(8,128)(2,1)S(1)}) fusion(bf16[512,256]{0,1:T(8,128)(2,1)S(1)} %get-tuple-element.44, bf16[512,2048]{1,0:T(8,128)(2,1)} %all-gather.5.cloned.1.call-done), kind=kOutput, calls=%fused_computation.12 | convolution fusion | flops 538966016 | bytes 3416064 | tf_op jit(solution)/shard_map/dot_general | solution.py:66
  122.9 1.7 multiply_reduce_fusion.1
  124.6 6.5 %all-reduce.2 = (bf16[512]{0:T(512)(128)(2,1)S(1)}, f32[1,2048]{1,0:T(1,128)}, f32[1,2048]{1,0:T(1,128)}) all-reduce(f32[512]{0:T(512)S(1)} %get-tuple-element.43, f32[1,2048]{1,0:T(1,128)S(1)} %bitcast.54, f32[1,2048]{1,0:T(1,128)S(1)} %bitcast.55), channel_id=1, replica_groups=mesh['ep'=16,'tp'=2] {'tp'}, use_global_device_ids=true, to_apply=%region_6.7 | all-reduce | flops 4608 | bytes 35840 | tf_op jit(solution)/shard_map/psum | solution.py:84
  131.2 13.0 %all_to_all.59 = bf16[16,32,1]{1,2,0:T(2,128)(2,1)S(1)} all-to-all(bf16[16,32,1]{1,2,0:T(2,128)(2,1)S(1)} %all_to_all.50), channel_id=1, replica_groups=mesh['ep'=16,'tp'=2] {'ep'}, dimensions={0} | all-to-all | bytes 2048 | tf_op jit(solution)/shard_map/all_to_all | solution.py:87
  144.2 8.7 %reduce-scatter.2.cloned.1.call-done = bf16[512,1024]{1,0:T(8,128)(2,1)} async-done(((bf16[512,2048]{1,0:T(8,128)(2,1)}), bf16[512,1024]{1,0:T(8,128)(2,1)}) %reduce-scatter.2.cloned.1.call-update) | async-done | bytes 1048592 | tf_op jit(solution)/shard_map/reduce_scatter | solution.py:78
  152.9 6.5 %all-to-all-start.3 = ((bf16[16,32,1024]{2,1,0:T(8,128)(2,1)}), bf16[16,32,1024]{2,1,0:T(8,128)(2,1)S(1)}, u32[]{:S(2)}, u32[]{:S(2)}) async-start(bf16[16,32,1024]{2,1,0:T(8,128)(2,1)} %bitcast.51), calls=%async_computation.4 | async-start | bytes 2097152 | tf_op jit(solution)/shard_map/all_to_all | solution.py:86
  159.4 2.3 %copy.39 = bf16[1,2048,256]{2,1,0:T(8,128)(2,1)} copy(bf16[1,2048,256]{1,2,0:T(8,128)(2,1)} %bitcast.53) | data formatting | bytes 2097152
  161.7 1.3 copy.38
  163.0 4.2 %multiply_reduce_fusion = (f32[256]{0:T(256)}, bf16[256,2048]{1,0:T(8,128)(2,1)}) fusion(bf16[512,2048]{0,1:T(8,128)(2,1)} %bitcast.50, f32[512]{0:T(512)S(1)} %reshape.88, f32[512,256]{0,1:T(8,128)} %copy-done.10, f32[512,256]{0,1:T(8,128)} %copy-done.9), kind=kOutput, calls=%fused_computation.10 | convolution fusion | flops 539885312 | bytes 4197376 | tf_op jit(solution)/shard_map/dot_general | solution.py:63
  167.3 1.9 gather_fusion.3
  170.0 14.3 %all-to-all-done.3 = bf16[16,32,1024]{2,1,0:T(8,128)(2,1)S(1)} async-done(((bf16[16,32,1024]{2,1,0:T(8,128)(2,1)}), bf16[16,32,1024]{2,1,0:T(8,128)(2,1)S(1)}, u32[]{:S(2)}, u32[]{:S(2)}) %all-to-all-start.3) | async-done | bytes 1048608 | tf_op jit(solution)/shard_map/all_to_all | solution.py:86
  184.3 1.2 gather_fusion.2
  185.7 2.1 %reduce_sum.58 = bf16[128,1024]{1,0:T(8,128)(2,1)} reduce(bf16[128,2,1024]{2,1,0:T(2,128)(2,1)S(1)} %gather.17, bf16[]{:T(256)} %constant.13.clone.1), dimensions={1}, to_apply=%region_4.5 | reduce | flops 131072 | bytes 786434 | tf_op jit(solution)/shard_map/reduce_sum | solution.py:92
  (58 shorter events, 8.2 us)
Async XLA Ops:
  7.2 105.4 %copy-start = (bf16[1,2048,256]{2,1,0:T(8,128)(2,1)S(1)}, bf16[1,2048,256]{2,1,0:T(8,128)(2,1)}, u32[]{:S(2)}) copy-start(bf16[1,2048,256]{2,1,0:T(8,128)(2,1)} %param.11) | copy-start | bytes 3145732
  7.2 82.1 %all-gather.3.cloned.1.call-start = ((), (), s32[]{:S(2)}) async-start(), calls=%async_computation.6 | async-start | bytes 3145728 | tf_op jit(solution)/shard_map/all_gather | solution.py:42
  45.9 66.7 %all-gather.5.cloned.1.call-start = ((), (), s32[]{:S(2)}) async-start(), calls=%async_computation.7 | async-start | bytes 3145728 | tf_op jit(solution)/shard_map/all_gather | solution.py:41
  48.0 29.7 %copy-start.5 = (bf16[128,2]{0,1:T(2,128)(2,1)S(1)}, bf16[128,2]{0,1:T(2,128)(2,1)}, u32[]{:S(2)}) copy-start(bf16[128,2]{0,1:T(2,128)(2,1)} %param.9) | copy-start | bytes 1540
  77.7 75.2 %reduce-scatter.2.cloned.1.call-start = ((), (), s32[]{:S(2)}) async-start(), calls=%async_computation.8 | async-start | bytes 3145728 | tf_op jit(solution)/shard_map/reduce_scatter | solution.py:78
  92.2 23.7 %copy-start.1 = (bf16[2,512,1024]{1,2,0:T(8,128)(2,1)}, bf16[2,512,1024]{1,2,0:T(8,128)(2,1)S(1)}, u32[]{:S(2)}) copy-start(bf16[2,512,1024]{1,2,0:T(8,128)(2,1)S(1)} %copy.35) | copy-start | bytes 6291460
  112.6 2.5 %copy-start.2 = (bf16[1,2048,256]{2,1,0:T(8,128)(2,1)S(1)}, bf16[1,2048,256]{2,1,0:T(8,128)(2,1)}, u32[]{:S(2)}) copy-start(bf16[1,2048,256]{2,1,0:T(8,128)(2,1)} %param.12) | copy-start | bytes 3145732
  112.6 2.5 %copy-start.6 = (bf16[512,2048]{1,0:T(8,128)(2,1)S(1)}, bf16[512,2048]{1,0:T(8,128)(2,1)}, u32[]{:S(2)}) copy-start(bf16[512,2048]{1,0:T(8,128)(2,1)} %all-gather.5.cloned.1.call-done) | copy-start | bytes 6291460
  115.2 2.3 %copy-start.9 = (f32[512,256]{0,1:T(8,128)}, f32[512,256]{0,1:T(8,128)S(1)}, u32[]{:S(2)}) copy-start(f32[512,256]{0,1:T(8,128)S(1)} %fusion.3) | copy-start | bytes 1572868
  115.2 1.4 copy-start.8
  115.9 1.6 copy-start.10
  117.5 0.8 copy-start.3
  120.4 2.5 %copy-start.4 = (bf16[512,256]{0,1:T(8,128)(2,1)S(1)}, bf16[512,256]{0,1:T(8,128)(2,1)}, u32[]{:S(2)}) copy-start(bf16[512,256]{0,1:T(8,128)(2,1)} %copy-done.3) | copy-start | bytes 786436
  120.4 2.5 %copy-start.7 = (bf16[512,2048]{1,0:T(8,128)(2,1)S(1)}, bf16[512,2048]{1,0:T(8,128)(2,1)}, u32[]{:S(2)}) copy-start(bf16[512,2048]{1,0:T(8,128)(2,1)} %all-gather.5.cloned.1.call-done) | copy-start | bytes 6291460
  152.9 31.4 %all-to-all-start.3 = ((bf16[16,32,1024]{2,1,0:T(8,128)(2,1)}), bf16[16,32,1024]{2,1,0:T(8,128)(2,1)S(1)}, u32[]{:S(2)}, u32[]{:S(2)}) async-start(bf16[16,32,1024]{2,1,0:T(8,128)(2,1)} %bitcast.51), calls=%async_computation.4 | async-start | bytes 2097152 | tf_op jit(solution)/shard_map/all_to_all | solution.py:86
Sparse Core Ops, SparseCore 0:
  46.0 31.9 all-gather.2
  79.5 33.0 all-gather.4
  120.5 32.2 reduce-scatter.1
